TPU v7x, 32 devices: a whole 2x2x4 slice. The times are simulated.
32 devices in a mesh: sp: 8 (over z, x), tp: 4 (over y, core).
Axes of the slice: x: 2, y: 2, z: 4, core: 2. Of those that a mesh axis runs over, the one named last changes fastest.
Arguments:
- residual: bfloat16 [6144, 2048], P('sp'), may hold values from -6 to 6
- query_matrix: bfloat16 [6144, 1024], P('sp', 'tp'), may hold values from -6 to 6
- key_matrix: bfloat16 [6144, 1024], P('sp', 'tp'), may hold values from -6 to 6
- value_matrix: bfloat16 [6144, 2048], P('sp', 'tp'), may hold values from -6 to 6
- output_gate_logit: bfloat16 [6144, 2048], P('sp', 'tp'), may hold values from -6 to 6
- input_gate_log: float32 [6144, 8], P('sp', 'tp'), may hold values from -4 to 125
- forget_gate_logit: float32 [6144, 8], P('sp', 'tp')
- extra_head_decay: float32 [6144, 8], P('sp', 'tp'), may hold values from -1 to 0
- head_norm_gain: float32 [2048], P('tp'), may hold values from 0.1 to 1.9
- projection: bfloat16 [2048, 2048], P('tp'), may hold values from -5.303301 to 5.303301
- cell_output_gain: float32 [2048], replicated, may hold values from 0.1 to 1.9
- mixer_input_gain: float32 [2048], replicated, may hold values from 0.1 to 1.9
- mixer_gate_weight: bfloat16 [2048, 5120], P('sp', 'tp'), may hold values from -0.125 to 0.125
- mixer_up_weight: bfloat16 [2048, 5120], P('sp', 'tp'), may hold values from -0.125 to 0.125
- mixer_down_weight: bfloat16 [5120, 2048], P('tp', 'sp'), may hold values from -0.078125 to 0.078125
Outputs:
- updated: bfloat16 [6144, 2048], P('sp', 'tp')
All inputs are finite; a program needn't handle non-finite values.
Results may differ from a plain program's by a relative error of at most 0.014.
Values may be sent and summed in bfloat16 or wider, within the bound.
A program may use at most 128 MiB of HBM per device.

v0:
```python
import jax
import jax.numpy as jnp
from jax import lax
from jax.sharding import PartitionSpec as P

DQK = 128
DV = 256
HIGHEST = lax.Precision.HIGHEST
EPSILON = 1e-06
LOWEST_LOG = -1e30


def carried_in(value, axis, join, neutral):
    count, mine = (lax.axis_size(axis), lax.axis_index(axis))
    pieces = jax.tree.map(lambda part: lax.all_gather(part, axis), value)
    subtotal = jax.tree.map(
        lambda part, zero: jnp.full_like(part, 0) + jnp.asarray(zero, part.dtype), value, neutral
    )

    def turn(position, subtotal):
        longer = join(subtotal, jax.tree.map(lambda part: part[position], pieces))
        return jax.tree.map(lambda new, old: jnp.where(position < mine, new, old), longer, subtotal)

    return lax.fori_loop(0, count - 1, turn, subtotal)


def heads_first(array, heads, width):
    return array.reshape(array.shape[0], heads, width).transpose(1, 0, 2)


def read_out(
    query_low, key_low, value_low, in_logs, running_log_total, memory, normalizer, stabilizer
):
    length = query_low.shape[1]
    causal = lax.broadcasted_iota(jnp.int32, (length, length), 0) >= lax.broadcasted_iota(
        jnp.int32, (length, length), 1
    )
    spread = running_log_total[:, :, None] - running_log_total[:, None, :] + in_logs[:, None, :]
    spread = jnp.where(causal[None], spread, -jnp.inf)
    carried = running_log_total + stabilizer[:, None]
    running = jnp.maximum(carried, jnp.max(spread, axis=-1))
    scores = jnp.einsum(
        "htd,hsd->hts", query_low, key_low, preferred_element_type=jnp.float32
    ) * DQK ** (-0.5)
    weights = jnp.exp(spread - running[:, :, None]) * scores
    scaled = jnp.exp(carried - running)
    scaled_query = query_low.astype(jnp.float32) * DQK ** (-0.5)
    numerator = jnp.einsum(
        "hts,hsv->htv", weights.astype(jnp.bfloat16), value_low, preferred_element_type=jnp.float32
    )
    numerator = numerator + scaled[:, :, None] * jnp.einsum(
        "hvd,htd->htv", memory, scaled_query, precision=HIGHEST
    )
    denominator = jnp.sum(weights, axis=-1) + scaled * jnp.einsum(
        "hd,htd->ht", normalizer, scaled_query, precision=HIGHEST
    )
    return numerator / jnp.maximum(jnp.abs(denominator), jnp.exp(-running))[:, :, None]


def fold_state(keyed, valued, in_logs, running_log_total, memory, normalizer, stabilizer):
    last = running_log_total[:, -1]
    lifted = last[:, None] - running_log_total + in_logs
    new_max = jnp.maximum(last + stabilizer, jnp.max(lifted, axis=-1))
    weights = jnp.exp(lifted - new_max[:, None])
    retained = jnp.exp(last + stabilizer - new_max)
    memory = retained[:, None, None] * memory + jnp.einsum(
        "hsv,hsd->hvd", weights[:, :, None] * valued, keyed, precision=HIGHEST
    )
    normalizer = retained[:, None] * normalizer + jnp.einsum(
        "hs,hsd->hd", weights, keyed, precision=HIGHEST
    )
    return (memory, normalizer, new_max)


def join_states(earlier, later):
    early_decay, early_memory, early_normalizer, early_max = earlier
    late_decay, late_memory, late_normalizer, late_max = later
    joined_max = jnp.maximum(late_decay + early_max, late_max)
    first_scale = jnp.exp(late_decay + early_max - joined_max)
    second_scale = jnp.exp(late_max - joined_max)
    memory = first_scale[:, None, None] * early_memory + second_scale[:, None, None] * late_memory
    normalizer = first_scale[:, None] * early_normalizer + second_scale[:, None] * late_normalizer
    return (early_decay + late_decay, memory, normalizer, joined_max)


def body(
    residual,
    query_matrix,
    key_matrix,
    value_matrix,
    output_gate_logit,
    input_gate_log,
    forget_gate_logit,
    extra_head_decay,
    head_norm_gain,
    projection,
    cell_output_gain,
    mixer_input_gain,
    mixer_gate_weight,
    mixer_up_weight,
    mixer_down_weight,
):
    tok_rows = residual.shape[0]
    width = residual.shape[1]
    heads_here = input_gate_log.shape[1]
    query_low = heads_first(query_matrix, heads_here, DQK)
    key_low = heads_first(key_matrix, heads_here, DQK)
    value_low = heads_first(value_matrix, heads_here, DV)
    keyed = key_low.astype(jnp.float32)
    valued = value_low.astype(jnp.float32)
    in_logs = input_gate_log.T
    running_log_total = jnp.cumsum(
        (jax.nn.log_sigmoid(forget_gate_logit) + extra_head_decay).T, axis=-1
    )
    zero_memory = jnp.zeros((heads_here, DV, DQK), jnp.float32)
    zero_normalizer = jnp.zeros((heads_here, DQK), jnp.float32)
    lowest = jnp.full((heads_here,), LOWEST_LOG, jnp.float32)
    local_memory, local_normalizer, local_max = fold_state(
        keyed, valued, in_logs, running_log_total, zero_memory, zero_normalizer, lowest
    )
    prior_decay, prior_memory, prior_normalizer, prior_max = carried_in(
        (running_log_total[:, -1], local_memory, local_normalizer, local_max),
        "sp",
        join_states,
        (jnp.zeros_like(lowest), zero_memory, zero_normalizer, lowest),
    )
    start_max = jnp.maximum(prior_decay, prior_max)
    lift = jnp.exp(prior_max - start_max)
    cells = read_out(
        query_low,
        key_low,
        value_low,
        in_logs,
        running_log_total,
        lift[:, None, None] * prior_memory,
        lift[:, None] * prior_normalizer,
        start_max,
    )
    centered = cells - jnp.mean(cells, axis=-1, keepdims=True)
    normed = centered * lax.rsqrt(jnp.mean(centered * centered, axis=-1, keepdims=True) + EPSILON)
    normed = normed * head_norm_gain.reshape(heads_here, DV)[:, None, :]
    normed = normed.transpose(1, 0, 2).reshape(tok_rows, heads_here * DV)
    gated = (normed * jax.nn.sigmoid(output_gate_logit.astype(jnp.float32))).astype(jnp.bfloat16)
    cols_here = width // lax.axis_size("tp")
    offset = lax.axis_index("tp") * cols_here
    columns = projection
    mixed = (
        lax.psum_scatter(
            lax.dot_general(
                columns, gated, (((0,), (1,)), ((), ())), preferred_element_type=jnp.float32
            ).astype(jnp.bfloat16),
            "tp",
            scatter_dimension=0,
            tiled=True,
        )
        .astype(jnp.float32)
        .T
    )
    squares = lax.psum(jnp.sum(mixed * mixed, axis=-1), "tp")
    mixed = (
        mixed
        * lax.rsqrt(squares / width + EPSILON)[:, None]
        * lax.dynamic_slice_in_dim(cell_output_gain, offset, cols_here, 0)
    )
    own_residual = lax.dynamic_slice_in_dim(residual, offset, cols_here, 1).astype(jnp.float32)
    first_sum = (own_residual + mixed).astype(jnp.bfloat16)
    own_first = lax.optimization_barrier(first_sum).astype(jnp.float32)
    first_total = lax.psum(jnp.sum(own_first * own_first, axis=-1), "tp")
    own_gain = lax.dynamic_slice_in_dim(mixer_input_gain, offset, cols_here, 0)
    normed_own = (own_first * lax.rsqrt(first_total / width + EPSILON)[:, None] * own_gain).astype(
        jnp.bfloat16
    )
    normed_rows = lax.all_gather(normed_own, "tp", axis=1, tiled=True)
    columns = normed_rows
    gate_value = jnp.dot(
        columns,
        lax.all_gather(mixer_gate_weight, "sp", axis=0, tiled=True),
        preferred_element_type=jnp.float32,
    )
    up_value = jnp.dot(
        columns,
        lax.all_gather(mixer_up_weight, "sp", axis=0, tiled=True),
        preferred_element_type=jnp.float32,
    )
    activated = (jax.nn.silu(gate_value) * up_value).astype(jnp.bfloat16)
    down_terms = jnp.dot(
        activated,
        lax.all_gather(mixer_down_weight, "sp", axis=1, tiled=True),
        preferred_element_type=jnp.float32,
    )
    channel_out = lax.psum_scatter(
        down_terms.astype(jnp.bfloat16), "tp", scatter_dimension=1, tiled=True
    ).astype(jnp.float32)
    return (own_first + 0.5 * channel_out).astype(jnp.bfloat16)


def solution(mesh):
    return jax.shard_map(
        body,
        mesh=mesh,
        in_specs=(
            P("sp", None),
            P("sp", "tp"),
            P("sp", "tp"),
            P("sp", "tp"),
            P("sp", "tp"),
            P("sp", "tp"),
            P("sp", "tp"),
            P("sp", "tp"),
            P("tp"),
            P("tp", None),
            P(),
            P(),
            P("sp", "tp"),
            P("sp", "tp"),
            P("tp", "sp"),
        ),
        out_specs=P("sp", "tp"),
        check_vma=False,
    )
```

profile of v0, /device:TPU:0, one launch (start us, length us, event | category | flops | bytes accessed | tf_op | source)
XLA Modules:
  0.0 489.8 jit_solution(3324282672585852311)
XLA Ops:
  6.6 0.9 fusion.53
  7.5 0.6 reduce-window.6
  8.1 0.2 slice_reduce_fusion
  8.2 0.2 reduce-window.9
  8.5 0.2 slice_reduce_fusion.1
  8.7 0.9 fusion.71
  9.6 0.1 copy.41
  9.7 0.2 multiply_reduce_fusion.1
  9.9 1.4 copy.54
  11.3 0.1 subtract_exponential_fusion.3
  11.4 2.8 fusion.32
  14.4 0.6 dynamic-slice
  15.5 0.2 dynamic-update-slice
  15.8 22.4 %all-gather.3 = f32[8,1,2]{2,1,0:T(1,128)S(1)} all-gather(f32[1,1,2]{2,1,0:T(1,128)S(1)} %fusion.59), channel_id=1, replica_groups=mesh['sp'=8,'tp'=4] {'sp'}, dimensions={0}, use_global_device_ids=true | all-gather | bytes 72 | tf_op jit(solution)/shard_map/all_gather | solution.py:15
  38.1 17.6 %all-reduce = f32[16]{0:T(128)S(1)} all-reduce(f32[16]{0:T(128)S(1)} %dynamic-update-slice), channel_id=2, replica_groups=mesh['sp'=8,'tp'=4] {'sp'}, use_global_device_ids=true, to_apply=%add | all-reduce | flops 16 | bytes 128
  55.9 0.3 fusion.40
  56.2 18.9 %all-gather.4 = f32[8,2,128]{2,1,0:T(2,128)S(1)} all-gather(f32[1,2,128]{2,1,0:T(2,128)S(1)} %add_bitcast_fusion.1), channel_id=4, replica_groups=mesh['sp'=8,'tp'=4] {'sp'}, dimensions={0}, use_global_device_ids=true | all-gather | bytes 9216 | tf_op jit(solution)/shard_map/all_gather | solution.py:15
  75.2 0.2 iota_compare_fusion
  75.4 0.9 fusion.7
  76.4 8.3 %while.20 = (s32[]{:T(128)}, f32[2]{0:T(128)S(1)}, f32[2,256,128]{2,1,0:T(8,128)S(1)}, f32[2,128]{1,0:T(2,128)S(1)}, f32[2]{0:T(128)S(1)}, /*index=5*/s32[]{:T(1...) while((s32[]{:T(128)}, f32[2]{0:T(128)S(1)}, ...), condition=%wide.region_4.5_spmd.clone, body=%wide.region_3.4_spmd.clone.sunk | while | flops 328984 | bytes 789781 | solution.py:24
  76.4 1.1 fusion.90
  77.5 0.1 fusion.91
  77.6 1.1 fusion.90
  78.7 0.1 fusion.91
  78.8 1.1 fusion.90
  79.9 0.1 fusion.91
  80.0 1.1 fusion.90
  81.0 0.1 fusion.91
  81.2 1.1 fusion.90
  82.2 0.1 fusion.91
  82.4 1.1 fusion.90
  83.4 0.1 fusion.91
  83.5 1.1 fusion.90
  84.6 0.1 fusion.91
  84.8 3.0 fusion.10
  87.8 0.7 fusion.36
  88.5 1.5 fusion.37
  90.0 0.1 fusion.56
  90.1 2.4 fusion.69
  92.5 0.3 multiply_reduce_fusion
  92.9 1.5 fusion.28
  94.4 3.1 copy.47
  97.5 4.9 fusion.9
  102.5 0.7 all-gather.13.cloned.1.call-update
  103.2 0.8 dynamic_slice.38
  104.0 0.8 dynamic_slice.39
  104.7 32.8 %reduce-scatter.3.cloned.1.call-done = bf16[512,768]{0,1:T(8,128)(2,1)} async-done(((bf16[2048,768]{0,1:T(8,128)(2,1)}), bf16[512,768]{0,1:T(8,128)(2,1)}) %reduce-scatter.3.cloned.1.call-update) | async-done | bytes 786448 | tf_op jit(solution)/shard_map/reduce_scatter | solution.py:148
  137.6 1.4 fusion.15
  138.9 5.8 %psum.14 = f32[768]{0:T(1024)S(1)} all-reduce(f32[768]{0:T(1024)S(1)} %fusion.15), channel_id=1, replica_groups=mesh['sp'=8,'tp'=4] {'tp'}, use_global_device_ids=true, to_apply=%region_11.12 | all-reduce | flops 768 | bytes 6144 | tf_op jit(solution)/shard_map/psum | solution.py:159
  144.7 1.7 fusion.19
  146.4 0.2 fusion.20
  146.7 5.7 %psum.15 = f32[768]{0:T(1024)S(1)} all-reduce(f32[768]{0:T(1024)S(1)} %fusion.20), channel_id=1, replica_groups=mesh['sp'=8,'tp'=4] {'tp'}, use_global_device_ids=true, to_apply=%region_13.14 | all-reduce | flops 768 | bytes 6144 | tf_op jit(solution)/shard_map/psum | solution.py:168
  152.3 1.1 fusion.22
  153.5 0.5 all-gather.15.cloned.1.call-update
  154.1 0.5 all-gather.17.cloned.1.call-update
  154.7 0.3 reduce-scatter.5.cloned.1.call-start
  154.9 70.8 %all-gather.13.cloned.1.call-done = bf16[2048,1280]{1,0:T(8,128)(2,1)} async-done(((bf16[256,1280]{1,0:T(8,128)(2,1)}), bf16[2048,1280]{1,0:T(8,128)(2,1)}) %all-gather.13.cloned.1.call-update) | async-done | bytes 5242896 | tf_op jit(solution)/shard_map/all_gather | solution.py:177
  225.7 28.1 %all-gather.11.cloned.1.call-done = bf16[768,2048]{1,0:T(8,128)(2,1)} async-done(((bf16[768,512]{1,0:T(8,128)(2,1)}), bf16[768,2048]{1,0:T(8,128)(2,1)}) %all-gather.11.cloned.1.call-update) | async-done | bytes 3145744 | tf_op jit(solution)/shard_map/all_gather | solution.py:173
  253.8 9.6 %fusion.72 = f32[768,1280]{1,0:T(8,128)} fusion(bf16[768,2048]{1,0:T(8,128)(2,1)} %all-gather.11.cloned.1.call-done, bf16[2048,1280]{1,0:T(8,128)(2,1)} %all-gather.13.cloned.1.call-done), kind=kOutput, calls=%fused_computation.118 | convolution fusion | flops 4026531840 | bytes 12320768 | tf_op jit(solution)/shard_map/dot_general | solution.py:175
  263.4 78.4 %all-gather.15.cloned.1.call-done = bf16[2048,1280]{1,0:T(8,128)(2,1)} async-done(((bf16[256,1280]{1,0:T(8,128)(2,1)}), bf16[2048,1280]{1,0:T(8,128)(2,1)}) %all-gather.15.cloned.1.call-update) | async-done | bytes 5242896 | tf_op jit(solution)/shard_map/all_gather | solution.py:182
  341.8 86.9 %all-gather.17.cloned.1.call-done = bf16[1280,2048]{1,0:T(8,128)(2,1)} async-done(((bf16[1280,256]{1,0:T(8,128)(2,1)}), bf16[1280,2048]{1,0:T(8,128)(2,1)}) %all-gather.17.cloned.1.call-update) | async-done | bytes 5242896 | tf_op jit(solution)/shard_map/all_gather | solution.py:188
  428.7 16.0 %convolution_convert_fusion.1 = bf16[768,2048]{1,0:T(8,128)(2,1)} fusion(bf16[1280,2048]{1,0:T(8,128)(2,1)} %all-gather.17.cloned.1.call-done, bf16[768,2048]{1,0:T(8,128)(2,1)} %all-gather.11.cloned.1.call-done, bf16[2048,1280]{1,0:T(8,128)(2,1)} %all-gather.15.cloned.1.call-done, f32[768,1280]{1,0:T(8,128)} %fusion.72), kind=kOutput, calls=%fused_computation.23 | convolution fusion | flops 8060534784 | bytes 20709376 | tf_op jit(solution)/shard_map/dot_general | solution.py:186
  444.7 36.1 %reduce-scatter.5.cloned.1.call-done = bf16[768,512]{1,0:T(8,128)(2,1)} async-done(((bf16[768,2048]{1,0:T(8,128)(2,1)}), bf16[768,512]{1,0:T(8,128)(2,1)}) %reduce-scatter.5.cloned.1.call-update) | async-done | bytes 786448 | tf_op jit(solution)/shard_map/reduce_scatter | solution.py:191
  480.7 2.2 fusion.23
  (64 shorter events, 1.1 us)
Async XLA Ops:
  6.5 91.0 %copy-start = (bf16[512,2048]{1,0:T(8,128)(2,1)S(1)}, bf16[512,2048]{1,0:T(8,128)(2,1)}, u32[]{:S(2)}) copy-start(bf16[512,2048]{1,0:T(8,128)(2,1)} %param.26) | copy-start | bytes 6291460
  6.5 7.8 %copy-start.8 = (u32[32]{0:T(128)S(1)}, u32[32]{0:T(128)}, u32[]{:S(2)}) copy-start(u32[32]{0:T(128)} %constant.77) | copy-start | bytes 388
  6.5 49.4 %copy-start.4 = (bf16[768,256]{1,0:T(8,128)(2,1)S(1)}, bf16[768,256]{1,0:T(8,128)(2,1)}, u32[]{:S(2)}) copy-start(bf16[768,256]{1,0:T(8,128)(2,1)} %param.19) | copy-start | bytes 1179652
  6.5 49.3 %copy-start.6 = (f32[512]{0:T(512)S(1)}, f32[512]{0:T(512)}, u32[]{:S(2)}) copy-start(f32[512]{0:T(512)} %param.25) | copy-start | bytes 6148
  6.5 69.8 %all-gather.19.cloned.1.call-start = ((), (), s32[]{:S(2)}) async-start(), calls=%async_computation.8 | async-start | bytes 2359296 | tf_op jit(solution)/shard_map/all_gather | solution.py:15
  7.5 67.9 %copy-start.5 = (f32[768,2]{0,1:T(2,128)S(1)}, f32[768,2]{0,1:T(2,128)}, u32[]{:S(2)}) copy-start(f32[768,2]{0,1:T(2,128)} %param.22) | copy-start | bytes 18436
  11.3 26.8 %copy-start.1 = (bf16[768,512]{0,1:T(8,128)(2,1)}, bf16[768,512]{0,1:T(8,128)(2,1)S(1)}, u32[]{:S(2)}) copy-start(bf16[768,512]{0,1:T(8,128)(2,1)S(1)} %copy.54) | copy-start | bytes 2359300
  14.3 123.3 %reduce-scatter.3.cloned.1.call-start = ((), (), s32[]{:S(2)}) async-start(), calls=%async_computation.2 | async-start | bytes 3932160 | tf_op jit(solution)/shard_map/reduce_scatter | solution.py:148
  75.4 9.4 %copy-start.3 = (bf16[768,256]{1,0:T(8,128)(2,1)S(1)}, bf16[768,256]{1,0:T(8,128)(2,1)}, u32[]{:S(2)}) copy-start(bf16[768,256]{1,0:T(8,128)(2,1)} %param.18) | copy-start | bytes 1179652
  87.7 2.4 copy-start.2
  94.4 3.1 copy-start.7
  102.4 123.3 %all-gather.13.cloned.1.call-start = ((), (), s32[]{:S(2)}) async-start(), calls=%async_computation.4 | async-start | bytes 5898240 | tf_op jit(solution)/shard_map/all_gather | solution.py:177
  103.2 150.7 %all-gather.11.cloned.1.call-start = ((), (), s32[]{:S(2)}) async-start(), calls=%async_computation.3 | async-start | bytes 3932160 | tf_op jit(solution)/shard_map/all_gather | solution.py:173
  153.5 188.3 %all-gather.15.cloned.1.call-start = ((), (), s32[]{:S(2)}) async-start(), calls=%async_computation.5 | async-start | bytes 5898240 | tf_op jit(solution)/shard_map/all_gather | solution.py:182
  154.1 274.6 %all-gather.17.cloned.1.call-start = ((), (), s32[]{:S(2)}) async-start(), calls=%async_computation.6 | async-start | bytes 5898240 | tf_op jit(solution)/shard_map/all_gather | solution.py:188
  154.7 326.0 %reduce-scatter.5.cloned.1.call-start = ((), (), s32[]{:S(2)}) async-start(), calls=%async_computation.7 | async-start | bytes 3932160 | tf_op jit(solution)/shard_map/reduce_scatter | solution.py:191
Sparse Core Ops, SparseCore 0:
  14.4 52.0 all-gather.18
  102.5 34.9 reduce-scatter.2
  139.8 85.8 all-gather.12
  227.1 26.6 all-gather.10
  255.9 85.8 all-gather.14
  343.7 84.9 all-gather.16
  444.8 35.8 reduce-scatter.4
where the time goes:
time: 491 us; the launch traced here: 490 us
  waiting for transfers between devices  335 us (68%)
  blocking collectives  70.3 us (14%)
  matrix products  41 us (8%)
  other arithmetic  21.3 us (4%)
  between operations  14.3 us (3%)
  local copies, waits for them, and re-layouts  7.45 us (2%)
    all_gather x1, waiting for transfers between devices, body(): lax.all_gather(mixer_down_weight, 'sp', axis=1, tiled=True)  86.9 us
    all_gather x1, waiting for transfers between devices, body(): lax.all_gather(mixer_up_weight, 'sp', axis=0, tiled=True)  78.4 us
    all_gather x1, waiting for transfers between devices, body(): lax.all_gather(mixer_gate_weight, 'sp', axis=0, tiled=True)  70.8 us
    all_gather x2, blocking collectives, carried_in(): pieces = jax.tree.map(lambda part: lax.all_gather(part, axis), value)  41.3 us
    reduce_scatter x1, waiting for transfers between devices, body(): lax.psum_scatter(down_terms.astype(jnp.bfloat16), 'tp', scatter_dimension...  36.1 us
    reduce_scatter x1, waiting for transfers between devices, body(): lax.psum_scatter(lax.dot_general(columns, gated, (((0,), (1,)), ((), ()))...  32.8 us
    all_gather x1, waiting for transfers between devices, body(): normed_rows = lax.all_gather(normed_own, 'tp', axis=1, tiled=True)  28.1 us
    unnamed x1, blocking collectives  17.6 us
  transfers between devices with their start and end apart: 7, of which 6 were waited for; matrix products, arithmetic and copies ran while one was open for 4% of the time, Pallas kernels for 0%

commit v1 on v0

--- a/solution.py
+++ b/solution.py
@@ -170,7 +170,12 @@
     normed_own = (own_first * lax.rsqrt(first_total / width + EPSILON)[:, None] * own_gain).astype(
         jnp.bfloat16
     )
-    normed_rows = lax.all_gather(normed_own, "tp", axis=1, tiled=True)
+    ring = [normed_own]
+    for hop in range(3):
+        ring.append(lax.ppermute(ring[-1], "tp", [(dev, (dev + 1) % 4) for dev in range(4)]))
+    normed_rows = jnp.roll(
+        jnp.concatenate(ring[::-1], axis=1), (lax.axis_index("tp") + 1) * ring[0].shape[1], axis=1
+    )
     columns = normed_rows
     gate_value = jnp.dot(
         columns,

time: 491 us -> 462 us (0.941)
  waiting for transfers between devices: 335 us -> 292 us
  local copies, waits for them, and re-layouts: 7.45 us -> 19 us
    all_gather x1, waiting for transfers between devices: 70.8 us -> 24.3 us  [body(): lax.all_gather(mixer_gate_weight, 'sp', axis=0, tiled=True)]
    ppermute x0 -> x3, waiting for transfers between devices: none -> 34.6 us  [body(): lax.ppermute(ring[-1], 'tp', [(dev, (dev + 1) % 4) for dev in range(4)])]
    all_gather x1 -> x0, waiting for transfers between devices: 28.1 us -> none  [body(): normed_rows = lax.all_gather(normed_own, 'tp', axis=1, tiled=True)]
    unnamed x22 -> x30, local copies, waits for them, and re-layouts: 0.87 us -> 12.5 us
  transfers between devices with their start and end apart: 7 -> 9, of which waited for: 6 -> 8; matrix products, arithmetic and copies ran while one was open for 4% -> 7% of each run, Pallas kernels for 0% -> 0%
where the time goes in v1:
time: 462 us; the launch traced here: 461 us
  waiting for transfers between devices  292 us (63%)
  blocking collectives  70.2 us (15%)
  matrix products  42.2 us (9%)
  other arithmetic  22.8 us (5%)
  local copies, waits for them, and re-layouts  19 us (4%)
  between operations  14.3 us (3%)
    all_gather x1, waiting for transfers between devices, body(): lax.all_gather(mixer_down_weight, 'sp', axis=1, tiled=True)  86.9 us
    all_gather x1, waiting for transfers between devices, body(): lax.all_gather(mixer_up_weight, 'sp', axis=0, tiled=True)  76.5 us
    all_gather x2, blocking collectives, carried_in(): pieces = jax.tree.map(lambda part: lax.all_gather(part, axis), value)  41.2 us
    reduce_scatter x1, waiting for transfers between devices, body(): lax.psum_scatter(down_terms.astype(jnp.bfloat16), 'tp', scatter_dimension...  36.1 us
    ppermute x3, waiting for transfers between devices, body(): lax.ppermute(ring[-1], 'tp', [(dev, (dev + 1) % 4) for dev in range(4)])  34.6 us
    reduce_scatter x1, waiting for transfers between devices, body(): lax.psum_scatter(lax.dot_general(columns, gated, (((0,), (1,)), ((), ()))...  31.7 us
    all_gather x1, waiting for transfers between devices, body(): lax.all_gather(mixer_gate_weight, 'sp', axis=0, tiled=True)  24.3 us
    unnamed x1, blocking collectives  17.6 us
  transfers between devices with their start and end apart: 9, of which 8 were waited for; matrix products, arithmetic and copies ran while one was open for 7% of the time, Pallas kernels for 0%

profile of v1, /device:TPU:0, one launch (start us, length us, event | category | flops | bytes accessed | tf_op | source)
XLA Modules:
  0.0 460.7 jit_solution(16166256015986355159)
XLA Ops:
  6.6 0.9 fusion.60
  7.5 0.6 reduce-window.6
  8.1 0.2 slice_reduce_fusion
  8.2 0.2 reduce-window.9
  8.5 0.2 slice_reduce_fusion.1
  8.7 0.9 fusion.81
  9.7 0.2 multiply_reduce_fusion.1
  9.9 1.4 copy.54
  11.4 2.8 fusion.37
  14.3 0.6 dynamic-slice
  15.5 0.2 dynamic-update-slice
  15.7 22.4 %all-gather.3 = f32[8,1,2]{2,1,0:T(1,128)S(1)} all-gather(f32[1,1,2]{2,1,0:T(1,128)S(1)} %fusion.66), channel_id=1, replica_groups=mesh['sp'=8,'tp'=4] {'sp'}, dimensions={0}, use_global_device_ids=true | all-gather | bytes 72 | tf_op jit(solution)/shard_map/all_gather | solution.py:15
  38.1 17.6 %all-reduce = f32[16]{0:T(128)S(1)} all-reduce(f32[16]{0:T(128)S(1)} %dynamic-update-slice), channel_id=2, replica_groups=mesh['sp'=8,'tp'=4] {'sp'}, use_global_device_ids=true, to_apply=%add | all-reduce | flops 16 | bytes 128
  55.9 1.3 fusion.47
  57.2 18.8 %all-gather.4 = f32[8,2,128]{2,1,0:T(2,128)S(1)} all-gather(f32[1,2,128]{2,1,0:T(2,128)S(1)} %add_bitcast_fusion.1), channel_id=4, replica_groups=mesh['sp'=8,'tp'=4] {'sp'}, dimensions={0}, use_global_device_ids=true | all-gather | bytes 9216 | tf_op jit(solution)/shard_map/all_gather | solution.py:15
  76.1 0.2 iota_compare_fusion
  76.3 0.9 fusion.7
  77.2 8.3 %while.20 = (s32[]{:T(128)}, f32[2]{0:T(128)S(1)}, f32[2,256,128]{2,1,0:T(8,128)S(1)}, f32[2,128]{1,0:T(2,128)S(1)}, f32[2]{0:T(128)S(1)}, /*index=5*/s32[]{:T(1...) while((s32[]{:T(128)}, f32[2]{0:T(128)S(1)}, ...), condition=%wide.region_4.5_spmd.clone, body=%wide.region_3.4_spmd.clone.sunk | while | flops 328984 | bytes 789781 | solution.py:24
  77.3 1.1 fusion.97
  78.5 1.1 fusion.97
  79.7 1.1 fusion.97
  80.9 1.1 fusion.97
  82.1 1.1 fusion.97
  83.2 1.1 fusion.97
  84.4 1.1 fusion.97
  85.7 3.0 fusion.15
  88.8 0.7 fusion.43
  89.5 1.5 fusion.44
  91.1 2.4 fusion.79
  93.5 0.3 multiply_reduce_fusion
  93.8 1.5 fusion.33
  95.4 3.0 copy.47
  98.4 4.9 %fusion.8 = bf16[2048,768]{0,1:T(8,128)(2,1)} fusion(bf16[512,2048]{1,0:T(8,128)(2,1)S(1)} %copy-done, f32[768,512]{1,0:T(8,128)} %copy.47, bf16[768,512]{1,0:T(8,128)(2,1)S(1)} %copy-done.8), kind=kOutput, calls=%fused_computation.23 | convolution fusion | flops 1614544896 | bytes 7602176 | tf_op jit(solution)/shard_map/dot_general | solution.py:149
  103.3 0.7 all-gather.10.cloned.1.call-update
  104.1 0.5 all-gather.12.cloned.1.call-update
  104.7 0.5 all-gather.14.cloned.1.call-update
  105.3 0.8 dynamic_slice.42
  106.0 0.8 dynamic_slice.43
  106.8 31.7 %reduce-scatter.3.cloned.1.call-done = bf16[512,768]{0,1:T(8,128)(2,1)} async-done(((bf16[2048,768]{0,1:T(8,128)(2,1)}), bf16[512,768]{0,1:T(8,128)(2,1)}) %reduce-scatter.3.cloned.1.call-update) | async-done | bytes 786448 | tf_op jit(solution)/shard_map/reduce_scatter | solution.py:148
  138.5 1.4 fusion.20
  139.8 5.8 %psum.14 = f32[768]{0:T(1024)S(1)} all-reduce(f32[768]{0:T(1024)S(1)} %fusion.20), channel_id=1, replica_groups=mesh['sp'=8,'tp'=4] {'tp'}, use_global_device_ids=true, to_apply=%region_11.12 | all-reduce | flops 768 | bytes 6144 | tf_op jit(solution)/shard_map/psum | solution.py:159
  145.6 1.7 fusion.24
  147.3 0.2 fusion.25
  147.5 5.7 %psum.15 = f32[768]{0:T(1024)S(1)} all-reduce(f32[768]{0:T(1024)S(1)} %fusion.25), channel_id=1, replica_groups=mesh['sp'=8,'tp'=4] {'tp'}, use_global_device_ids=true, to_apply=%region_13.14 | all-reduce | flops 768 | bytes 6144 | tf_op jit(solution)/shard_map/psum | solution.py:168
  153.2 0.3 fusion.27
  153.5 11.4 %collective-permute-done = bf16[768,512]{1,0:T(8,128)(2,1)S(1)} collective-permute-done((bf16[768,512]{1,0:T(8,128)(2,1)S(1)}, bf16[768,512]{1,0:T(8,128)(2,1)S(1)}, u32[]{:S(2)}, u32[]{:S(2)}) %collective-permute-start) | collective-permute-done | bytes 786464 | tf_op jit(solution)/shard_map/ppermute | solution.py:175
  164.9 0.9 copy-done.1
  165.8 11.5 %collective-permute-done.1 = bf16[768,512]{1,0:T(8,128)(2,1)} collective-permute-done((bf16[768,512]{1,0:T(8,128)(2,1)S(1)}, bf16[768,512]{1,0:T(8,128)(2,1)}, u32[]{:S(2)}, u32[]{:S(2)}) %collective-permute-start.1) | collective-permute-done | bytes 786464 | tf_op jit(solution)/shard_map/ppermute | solution.py:175
  177.4 11.7 %collective-permute-done.2 = bf16[768,512]{1,0:T(8,128)(2,1)} collective-permute-done((bf16[768,512]{1,0:T(8,128)(2,1)}, bf16[768,512]{1,0:T(8,128)(2,1)}, u32[]{:S(2)}, u32[]{:S(2)}) %collective-permute-start.2) | collective-permute-done | bytes 786464 | tf_op jit(solution)/shard_map/ppermute | solution.py:175
  189.1 2.2 constant_dynamic-update-slice_fusion.7
  191.2 2.2 constant_dynamic-update-slice_fusion.6
  193.4 1.1 constant_dynamic-update-slice_fusion.5
  194.5 1.3 constant_dynamic-update-slice_fusion.4
  195.8 2.1 constant_dynamic-update-slice_fusion.3
  197.9 2.1 constant_dynamic-update-slice_fusion.2
  200.0 1.0 constant_dynamic-update-slice_fusion.1
  201.1 1.2 constant_dynamic-update-slice_fusion
  202.3 24.3 %all-gather.10.cloned.1.call-done = bf16[2048,1280]{1,0:T(8,128)(2,1)} async-done(((bf16[256,1280]{1,0:T(8,128)(2,1)}), bf16[2048,1280]{1,0:T(8,128)(2,1)}) %all-gather.10.cloned.1.call-update) | async-done | bytes 5242896 | tf_op jit(solution)/shard_map/all_gather | solution.py:182
  226.6 9.6 %fusion.11 = f32[768,1280]{1,0:T(8,128)} fusion(bf16[2048,1280]{1,0:T(8,128)(2,1)} %all-gather.10.cloned.1.call-done, bf16[768,4096]{1,0:T(8,128)(2,1)} %constant_dynamic-update-slice_fusion, s32[]{:T(128)S(6)} %select_n.95), kind=kOutput, calls=%fused_computation.26 | convolution fusion | flops 4026531840 | bytes 12320772 | tf_op jit(solution)/shard_map/dot_general | solution.py:180
  236.2 76.5 %all-gather.12.cloned.1.call-done = bf16[2048,1280]{1,0:T(8,128)(2,1)} async-done(((bf16[256,1280]{1,0:T(8,128)(2,1)}), bf16[2048,1280]{1,0:T(8,128)(2,1)}) %all-gather.12.cloned.1.call-update) | async-done | bytes 5242896 | tf_op jit(solution)/shard_map/all_gather | solution.py:187
  312.7 86.9 %all-gather.14.cloned.1.call-done = bf16[1280,2048]{1,0:T(8,128)(2,1)} async-done(((bf16[1280,256]{1,0:T(8,128)(2,1)}), bf16[1280,2048]{1,0:T(8,128)(2,1)}) %all-gather.14.cloned.1.call-update) | async-done | bytes 5242896 | tf_op jit(solution)/shard_map/all_gather | solution.py:193
  399.6 16.0 %convolution_convert_fusion.1 = bf16[768,2048]{1,0:T(8,128)(2,1)} fusion(bf16[1280,2048]{1,0:T(8,128)(2,1)} %all-gather.14.cloned.1.call-done, f32[768,1280]{1,0:T(8,128)} %fusion.11, bf16[2048,1280]{1,0:T(8,128)(2,1)} %all-gather.12.cloned.1.call-done, bf16[768,4096]{1,0:T(8,128)(2,1)} %constant_dynamic-update-slice_fusion, s32[]{:T(128)S(6)} %select_n.95), kind=kOutput, calls=%fused_computation.22 | convolution fusion | flops 8060534784 | bytes 20709380 | tf_op jit(solution)/shard_map/dot_general | solution.py:191
  415.6 36.1 %reduce-scatter.5.cloned.1.call-done = bf16[768,512]{1,0:T(8,128)(2,1)} async-done(((bf16[768,2048]{1,0:T(8,128)(2,1)}), bf16[768,512]{1,0:T(8,128)(2,1)}) %reduce-scatter.5.cloned.1.call-update) | async-done | bytes 786448 | tf_op jit(solution)/shard_map/reduce_scatter | solution.py:196
  451.6 2.2 fusion.28
  (77 shorter events, 2.0 us)
Async XLA Ops:
  6.5 91.8 %copy-start = (bf16[512,2048]{1,0:T(8,128)(2,1)S(1)}, bf16[512,2048]{1,0:T(8,128)(2,1)}, u32[]{:S(2)}) copy-start(bf16[512,2048]{1,0:T(8,128)(2,1)} %param.26) | copy-start | bytes 6291460
  6.5 7.8 %copy-start.9 = (u32[32]{0:T(128)S(1)}, u32[32]{0:T(128)}, u32[]{:S(2)}) copy-start(u32[32]{0:T(128)} %constant.99) | copy-start | bytes 388
  6.5 69.7 %copy-start.6 = (f32[768,2]{0,1:T(2,128)S(1)}, f32[768,2]{0,1:T(2,128)}, u32[]{:S(2)}) copy-start(f32[768,2]{0,1:T(2,128)} %param.22) | copy-start | bytes 18436
  6.5 49.2 %copy-start.7 = (f32[512]{0:T(512)S(1)}, f32[512]{0:T(512)}, u32[]{:S(2)}) copy-start(f32[512]{0:T(512)} %param.25) | copy-start | bytes 6148
  6.5 70.7 %all-gather.16.cloned.1.call-start = ((), (), s32[]{:S(2)}) async-start(), calls=%async_computation.7 | async-start | bytes 2359296 | tf_op jit(solution)/shard_map/all_gather | solution.py:15
  11.3 26.8 %copy-start.3 = (bf16[768,512]{0,1:T(8,128)(2,1)}, bf16[768,512]{0,1:T(8,128)(2,1)S(1)}, u32[]{:S(2)}) copy-start(bf16[768,512]{0,1:T(8,128)(2,1)S(1)} %copy.54) | copy-start | bytes 2359300
  14.2 71.4 %copy-start.5 = (bf16[768,256]{1,0:T(8,128)(2,1)S(1)}, bf16[768,256]{1,0:T(8,128)(2,1)}, u32[]{:S(2)}) copy-start(bf16[768,256]{1,0:T(8,128)(2,1)} %param.18) | copy-start | bytes 1179652
  14.3 124.2 %reduce-scatter.3.cloned.1.call-start = ((), (), s32[]{:S(2)}) async-start(), calls=%async_computation.2 | async-start | bytes 3932160 | tf_op jit(solution)/shard_map/reduce_scatter | solution.py:148
  85.7 5.4 %copy-start.4 = (bf16[768,512]{0,1:T(8,128)(2,1)S(1)}, bf16[768,512]{0,1:T(8,128)(2,1)}, u32[]{:S(2)}) copy-start(bf16[768,512]{0,1:T(8,128)(2,1)} %copy-done.3) | copy-start | bytes 2359300
  93.8 4.6 copy-start.8
  103.3 123.3 %all-gather.10.cloned.1.call-start = ((), (), s32[]{:S(2)}) async-start(), calls=%async_computation.3 | async-start | bytes 5898240 | tf_op jit(solution)/shard_map/all_gather | solution.py:182
  104.0 208.7 %all-gather.12.cloned.1.call-start = ((), (), s32[]{:S(2)}) async-start(), calls=%async_computation.4 | async-start | bytes 5898240 | tf_op jit(solution)/shard_map/all_gather | solution.py:187
  104.6 295.0 %all-gather.14.cloned.1.call-start = ((), (), s32[]{:S(2)}) async-start(), calls=%async_computation.5 | async-start | bytes 5898240 | tf_op jit(solution)/shard_map/all_gather | solution.py:193
  105.2 346.4 %reduce-scatter.5.cloned.1.call-start = ((), (), s32[]{:S(2)}) async-start(), calls=%async_computation.6 | async-start | bytes 3932160 | tf_op jit(solution)/shard_map/reduce_scatter | solution.py:196
  153.5 11.5 %collective-permute-start = (bf16[768,512]{1,0:T(8,128)(2,1)S(1)}, bf16[768,512]{1,0:T(8,128)(2,1)S(1)}, u32[]{:S(2)}, u32[]{:S(2)}) collective-permute-start(bf16[768,512]{1,0:T(8,128)(2,1)S(1)} %fusion.27), channel_id=1, source_target_pairs={{0,1},{1,2},{2,3},{3,0},{4,5},{5,6},{6,7},{7,4},{8,9},{9,10},{10,1... | collective-permute-start | bytes 2359304 | tf_op jit(solution)/shard_map/ppermute | solution.py:175
  164.9 0.9 copy-start.1
  165.8 11.5 %collective-permute-start.1 = (bf16[768,512]{1,0:T(8,128)(2,1)S(1)}, bf16[768,512]{1,0:T(8,128)(2,1)}, u32[]{:S(2)}, u32[]{:S(2)}) collective-permute-start(bf16[768,512]{1,0:T(8,128)(2,1)S(1)} %collective-permute-done), channel_id=1, source_target_pairs={{0,1},{1,2},{2,3},{3,0},{4,5},{5,6},{6,7},{7,4},{8,9},{9,10},{10,1... | collective-permute-start | bytes 2359304 | tf_op jit(solution)/shard_map/ppermute | solution.py:175
  177.3 11.7 %collective-permute-start.2 = (bf16[768,512]{1,0:T(8,128)(2,1)}, bf16[768,512]{1,0:T(8,128)(2,1)}, u32[]{:S(2)}, u32[]{:S(2)}) collective-permute-start(bf16[768,512]{1,0:T(8,128)(2,1)} %collective-permute-done.1), channel_id=1, source_target_pairs={{0,1},{1,2},{2,3},{3,0},{4,5},{5,6},{6,7},{7,4},{8,9},{9,10},{10,1... | collective-permute-start | bytes 2359304 | tf_op jit(solution)/shard_map/ppermute | solution.py:175
  177.3 16.1 %copy-start.2 = (bf16[768,512]{1,0:T(8,128)(2,1)S(1)}, bf16[768,512]{1,0:T(8,128)(2,1)}, u32[]{:S(2)}) copy-start(bf16[768,512]{1,0:T(8,128)(2,1)} %copy-done.1) | copy-start | bytes 2359300
Sparse Core Ops, SparseCore 0:
  14.4 52.0 all-gather.15
  103.4 34.9 reduce-scatter.2
  140.6 85.8 all-gather.9
  228.6 84.0 all-gather.11
  314.6 84.9 all-gather.13
  415.7 35.9 reduce-scatter.4
